TPU v7x, 32 devices: a whole 2x2x4 slice. The times are simulated.
32 devices in a mesh: sp: 8 (over z, y), tp: 4 (over x, core).
Axes of the slice: x: 2, y: 2, z: 4, core: 2. Of those that a mesh axis runs over, the one named last changes fastest.
Arguments:
- gate_in: bfloat16 [4096, 2048], P('sp', 'tp'), may hold values from -6 to 6
- value_in: bfloat16 [4096, 2048], P('sp', 'tp'), may hold values from -6 to 6
- gate_out: bfloat16 [4096, 2048], P('sp', 'tp'), may hold values from -6 to 6
- conv_taps: float32 [3, 2048], P(None, 'tp'), may hold values from -3.5 to 3.5
- proj_weight: bfloat16 [2048, 2048], P('tp'), may hold values from -0.125 to 0.125
- residual: bfloat16 [4096, 2048], P(('sp', 'tp')), may hold values from -6 to 6
- norm_gain: float32 [2048], replicated, may hold values from 0.1 to 1.9
- routes: int32 [4096, 2], P('sp'), may hold values from 0 to 7, all different within a row; in each aligned block of 128 rows (0 to 127, 128 to 255, ...) at most 64 rows name the same one
- route_weight: float32 [4096, 2], P('sp'), may hold values from 0.1 to 0.9
- expert_gate: bfloat16 [8, 2048, 2048], P('sp', None, 'tp'), may hold values from -0.125 to 0.125
- expert_up: bfloat16 [8, 2048, 2048], P('sp', None, 'tp'), may hold values from -0.125 to 0.125
- expert_down: bfloat16 [8, 2048, 2048], P('sp', 'tp'), may hold values from -0.125 to 0.125
Outputs:
- layer_out: bfloat16 [4096, 2048], P(('sp', 'tp'))
Inputs may be any that keep to these rules, and one draw needn't show every extreme that they name: `routes`: A token's 2 experts differ. In each aligned block of 128 tokens no expert is named by more than 64 tokens, a bound that some block reaches.
All inputs are finite; a program needn't handle non-finite values.
Results may differ from a plain program's by a relative error of at most 0.012.
Values may be sent and summed in bfloat16 or wider, within the bound.
A program may use at most 128 MiB of HBM per device.

v0:
```python
import jax
import jax.numpy as jnp
from jax import lax
from jax.sharding import PartitionSpec as P


def passed_along(shard, axis, by):
    size = lax.axis_size(axis)
    pairs = [(i, i + by) for i in range(size) if 0 <= i + by < size]
    return lax.ppermute(shard, axis, pairs)


def rounded(values):
    return lax.optimization_barrier(values.astype(jnp.bfloat16)).astype(jnp.float32)


def slot_numbers(route_ids, block_rows, expert_count):
    block_count = route_ids.shape[0] // block_rows
    flat_ids = route_ids.reshape(block_count, block_rows * route_ids.shape[1])
    one_hot = (
        flat_ids[:, :, None] == jnp.arange(expert_count, dtype=jnp.int32)[None, None, :]
    ).astype(jnp.int32)
    before = jnp.cumsum(one_hot, axis=1) - one_hot
    return jnp.sum(before * one_hot, axis=2).reshape(route_ids.shape)


def normalize(hidden_rows, norm_gain):
    inverse = lax.rsqrt(jnp.mean(hidden_rows * hidden_rows, axis=-1, keepdims=True) + 1e-05)
    return (hidden_rows * inverse * norm_gain).astype(jnp.bfloat16)


def dispatch_rows(normed, route_ids, block_rows, expert_count, capacity):
    row_count = route_ids.shape[0]
    top_count = route_ids.shape[1]
    block_count = row_count // block_rows
    slots = slot_numbers(route_ids, block_rows, expert_count)
    row_ids = jnp.arange(row_count, dtype=jnp.int32)
    flat_index = ((row_ids // block_rows)[:, None] * expert_count + route_ids) * capacity + slots
    slot_token = (
        jnp.full((block_count * expert_count * capacity,), row_count, jnp.int32)
        .at[flat_index.reshape(-1)]
        .set(jnp.repeat(row_ids, top_count))
    )
    padded_rows = jnp.concatenate([normed, jnp.zeros((1, normed.shape[1]), jnp.bfloat16)], axis=0)
    outgoing = padded_rows[slot_token].reshape(block_count, expert_count, capacity, normed.shape[1])
    return (outgoing, slots)


def body(
    gate_in,
    value_in,
    gate_out,
    conv_taps,
    proj_weight,
    residual,
    norm_gain,
    routes,
    route_weight,
    expert_gate,
    expert_up,
    expert_down,
):
    tok_dev = gate_in.shape[0]
    model_width = residual.shape[1]
    tp_count = lax.axis_size("tp")
    groups = lax.axis_size("sp")
    quarter = residual.shape[0]
    top_count = routes.shape[1]
    capacity = 2 * quarter * top_count // groups
    tp_index = lax.axis_index("tp")
    first_own = tp_index * quarter
    prior_gate, prior_value = passed_along(
        (gate_in[tok_dev - 2 :], value_in[tok_dev - 2 :]), "sp", 1
    )
    product = gate_in.astype(jnp.float32) * value_in.astype(jnp.float32)
    prior_mix = prior_gate.astype(jnp.float32) * prior_value.astype(jnp.float32)
    padded = jnp.concatenate([prior_mix, product], axis=0)
    conv_sum = conv_taps[0] * padded[:-2] + conv_taps[1] * padded[1:-1] + conv_taps[2] * padded[2:]
    mixed_out = (gate_out.astype(jnp.float32) * conv_sum).astype(jnp.bfloat16)
    own_routes = lax.dynamic_slice_in_dim(routes, first_own, quarter, 0)
    own_weights = lax.dynamic_slice_in_dim(route_weight, first_own, quarter, 0)
    row_block = mixed_out
    summed = lax.psum_scatter(
        rounded(jnp.dot(row_block, proj_weight, preferred_element_type=jnp.float32)).astype(
            jnp.bfloat16
        ),
        "tp",
        scatter_dimension=0,
        tiled=True,
    ).astype(jnp.float32)
    my_rows = residual.astype(jnp.float32) + summed
    normed = normalize(my_rows, norm_gain)
    outgoing, own_slots = dispatch_rows(normed, own_routes, quarter, groups, capacity)
    own_arrived = lax.all_to_all(outgoing, "sp", split_axis=1, concat_axis=1, tiled=True)
    received = lax.all_gather(own_arrived, "tp", axis=0, tiled=True)
    flat_rows = received.reshape(tp_count * groups * capacity, model_width)
    gate_weight = expert_gate[0]
    up_weight = expert_up[0]
    down_weight = expert_down[0]
    row_block = flat_rows
    gate_pre = jnp.dot(row_block, gate_weight, preferred_element_type=jnp.float32)
    up_pre = jnp.dot(row_block, up_weight, preferred_element_type=jnp.float32)
    hidden = (jax.nn.silu(gate_pre) * up_pre).astype(jnp.bfloat16)
    expert_rows = lax.psum_scatter(
        rounded(jnp.dot(hidden, down_weight, preferred_element_type=jnp.float32)).astype(
            jnp.bfloat16
        ),
        "tp",
        scatter_dimension=0,
        tiled=True,
    )
    returned = lax.all_to_all(
        expert_rows.reshape(groups, capacity, model_width),
        "sp",
        split_axis=0,
        concat_axis=0,
        tiled=True,
    )
    flat_pick = own_routes * capacity + own_slots
    picked = returned.reshape(groups * capacity, model_width)[flat_pick]
    weighted = jnp.sum(own_weights[:, :, None] * picked.astype(jnp.float32), axis=1)
    return (my_rows + weighted).astype(jnp.bfloat16)


def solution(mesh):
    placed = (
        P("sp", "tp"),
        P("sp", "tp"),
        P("sp", "tp"),
        P(None, "tp"),
        P("tp", None),
        P(("sp", "tp"), None),
        P(),
        P("sp", None),
        P("sp", None),
        P("sp", None, "tp"),
        P("sp", None, "tp"),
        P("sp", "tp", None),
    )
    return jax.shard_map(
        body, mesh=mesh, in_specs=placed, out_specs=P(("sp", "tp"), None), check_vma=False
    )
```

profile of v0, /device:TPU:0, one launch (start us, length us, event | category | flops | bytes accessed | tf_op | source)
XLA Modules:
  0.0 337.2 jit_solution(5291792366952498572)
XLA Ops:
  6.5 0.9 slice.28
  7.4 5.0 %collective-permute-start = (bf16[2,512]{1,0:T(2,128)(2,1)S(1)}, bf16[2,512]{1,0:T(2,128)(2,1)S(1)}, u32[]{:S(2)}, u32[]{:S(2)}) collective-permute-start(bf16[2,512]{1,0:T(2,128)(2,1)S(1)} %slice.28), channel_id=1, source_target_pairs={{0,4},{4,8},{8,12},{12,16},{16,20},{20,24},{24,28},{1,5},{5,9},{9,... | collective-permute-start | bytes 6152 | tf_op jit(solution)/shard_map/ppermute | solution.py:10
  12.4 0.7 slice.29
  13.1 3.4 %collective-permute-start.1 = (bf16[2,512]{1,0:T(2,128)(2,1)S(1)}, bf16[2,512]{1,0:T(2,128)(2,1)S(1)}, u32[]{:S(2)}, u32[]{:S(2)}) collective-permute-start(bf16[2,512]{1,0:T(2,128)(2,1)S(1)} %slice.29), channel_id=1, source_target_pairs={{0,4},{4,8},{8,12},{12,16},{16,20},{20,24},{24,28},{1,5},{5,9},{9,... | collective-permute-start | bytes 6152 | tf_op jit(solution)/shard_map/ppermute | solution.py:10
  16.6 1.3 convert_multiply_fusion
  18.0 3.8 %convolution_convert_fusion.1 = bf16[512,2048]{1,0:T(8,128)(2,1)} fusion(bf16[512,2048]{1,0:T(8,128)(2,1)S(1)} %copy-done.6, f32[2,512]{1,0:T(2,128)S(1)} %convert_multiply_fusion.1, f32[512,512]{1,0:T(8,128)S(1)} %convert_multiply_fusion, bf16[512,512]{1,0:T(8,128)(2,1)} %param.14, f32[512]{0:T(512)S(1)} %bitcast.44, f32[512]{0:T(512)S(1)} %bitcast.45, ...), kind=kOutput, calls=%fused_computation.5 | convolution fusion | flops 1077411840 | bytes 5777408 | tf_op jit(solution)/shard_map/dot_general | solution.py:84
  21.9 0.7 constant_dynamic-slice_fusion
  22.7 0.1 eq.27
  22.9 0.6 reduce-window.6
  23.5 0.2 slice_reduce_fusion
  23.8 0.1 reshape.195
  24.1 0.1 reshape.196
  24.2 0.1 reshape.222
  24.4 1.4 scatter_custom_fusion
  25.8 29.2 %reduce-scatter.3.cloned.1.call-done = bf16[128,2048]{1,0:T(8,128)(2,1)} async-done(((bf16[512,2048]{1,0:T(8,128)(2,1)}), bf16[128,2048]{1,0:T(8,128)(2,1)}) %reduce-scatter.3.cloned.1.call-update) | async-done | bytes 524304 | tf_op jit(solution)/shard_map/reduce_scatter | solution.py:83
  55.0 1.3 multiply_reduce_fusion.1
  56.3 1.3 multiply_convert_fusion.1
  57.6 3.3 gather_fusion
  61.0 53.7 %all_to_all.10 = bf16[1,8,64,2048]{3,2,0,1:T(8,128)(2,1)} all-to-all(bf16[1,8,64,2048]{3,2,0,1:T(8,128)(2,1)} %bitcast.39), channel_id=1, replica_groups=mesh['sp'=8,'tp'=4] {'sp'}, dimensions={1} | all-to-all | bytes 4194304 | tf_op jit(solution)/shard_map/all_to_all | solution.py:94
  114.8 56.4 %all-gather.2.cloned.1.call-done = bf16[4,8,64,2048]{3,2,1,0:T(8,128)(2,1)} async-done(((bf16[1,8,64,2048]{3,2,1,0:T(8,128)(2,1)}), bf16[4,8,64,2048]{3,2,1,0:T(8,128)(2,1)}) %all-gather.2.cloned.1.call-update) | async-done | bytes 8388624 | tf_op jit(solution)/shard_map/all_gather | solution.py:95
  171.2 7.7 %fusion.2 = f32[2048,512]{1,0:T(8,128)S(1)} fusion(bf16[2048,2048]{1,0:T(8,128)(2,1)} %bitcast.47, bf16[1,2048,512]{2,1,0:T(8,128)(2,1)} %param.21), kind=kOutput, calls=%fused_computation.8 | convolution fusion | flops 4294967296 | bytes 14680064 | tf_op jit(solution)/shard_map/dot_general | solution.py:101
  178.9 5.2 %multiply_convert_fusion = bf16[2048,512]{1,0:T(8,128)(2,1)S(1)} fusion(f32[2048,512]{1,0:T(8,128)S(1)} %fusion.2, bf16[2048,2048]{1,0:T(8,128)(2,1)S(1)} %bitcast.48, bf16[1,2048,512]{2,1,0:T(8,128)(2,1)S(1)} %copy-done.7), kind=kOutput, calls=%fused_computation.4 | convolution fusion | flops 4301258752 | bytes 16777216 | tf_op jit(solution)/shard_map/dot_general | solution.py:102
  184.1 6.8 %convolution_convert_fusion = bf16[2048,2048]{1,0:T(8,128)(2,1)} fusion(bf16[2048,512]{1,0:T(8,128)(2,1)S(1)} %multiply_convert_fusion, bf16[1,512,2048]{2,1,0:T(8,128)(2,1)S(1)} %copy-done), kind=kOutput, calls=%fused_computation.3 | convolution fusion | flops 4299161600 | bytes 12582912 | tf_op jit(solution)/shard_map/dot_general | solution.py:105
  190.9 71.5 %reduce-scatter.5.cloned.1.call-done = bf16[512,2048]{1,0:T(8,128)(2,1)} async-done(((bf16[2048,2048]{1,0:T(8,128)(2,1)}), bf16[512,2048]{1,0:T(8,128)(2,1)}) %reduce-scatter.5.cloned.1.call-update) | async-done | bytes 2097168 | tf_op jit(solution)/shard_map/reduce_scatter | solution.py:104
  262.5 5.5 %all-to-all-start.1 = ((bf16[8,64,2048]{2,1,0:T(8,128)(2,1)}), bf16[8,64,2048]{2,1,0:T(8,128)(2,1)}, u32[]{:S(2)}, u32[]{:S(2)}) async-start(bf16[8,64,2048]{2,1,0:T(8,128)(2,1)} %bitcast.41), calls=%async_computation.3 | async-start | bytes 4194304 | tf_op jit(solution)/shard_map/all_to_all | solution.py:112
  268.0 0.1 reshape.212
  268.1 0.7 constant_dynamic-slice_fusion.1
  268.9 47.2 %all-to-all-done.1 = bf16[8,64,2048]{2,1,0:T(8,128)(2,1)} async-done(((bf16[8,64,2048]{2,1,0:T(8,128)(2,1)}), bf16[8,64,2048]{2,1,0:T(8,128)(2,1)}, u32[]{:S(2)}, u32[]{:S(2)}) %all-to-all-start.1) | async-done | bytes 2097184 | tf_op jit(solution)/shard_map/all_to_all | solution.py:112
  316.2 5.2 %gather_fusion.1 = bf16[256,2048]{1,0:T(8,128)(2,1)} fusion(bf16[512,2048]{1,0:T(8,128)(2,1)} %bitcast.18, s32[1024]{0:T(1024)S(1)} %pad_clamp_fusion), kind=kCustom, calls=%fused_computation.1 | custom fusion | bytes 2098176 | tf_op jit(solution)/shard_map/gather | solution.py:120
  321.4 3.4 %reshape.229 = f32[128,2,2048]{2,1,0:T(2,128)} reshape(bf16[256,2048]{1,0:T(8,128)(2,1)} %gather_fusion.1) | data formatting | bytes 3145728 | tf_op jit(solution)/shard_map/convert_element_type | solution.py:121
  324.8 4.9 %multiply_reduce_fusion = f32[128,2048]{1,0:T(8,128)S(1)} fusion(f32[128,2,2048]{2,1,0:T(2,128)} %reshape.229, f32[128,2]{1,0:T(8,128)S(1)} %copy.16), kind=kLoop, calls=%fused_computation.10 | loop fusion | flops 786432 | bytes 3146752 | tf_op jit(solution)/shard_map/reduce_sum | solution.py:121
  329.7 1.0 add_convert_fusion
  (41 shorter events, 0.7 us)
Async XLA Ops:
  6.5 177.6 %copy-start = (bf16[1,512,2048]{2,1,0:T(8,128)(2,1)S(1)}, bf16[1,512,2048]{2,1,0:T(8,128)(2,1)}, u32[]{:S(2)}) copy-start(bf16[1,512,2048]{2,1,0:T(8,128)(2,1)} %param.23) | copy-start | bytes 6291460
  6.5 11.4 %copy-start.4 = (f32[3,512]{1,0:T(4,128)S(1)}, f32[3,512]{1,0:T(4,128)}, u32[]{:S(2)}) copy-start(f32[3,512]{1,0:T(4,128)} %param.15) | copy-start | bytes 18436
  6.5 48.5 %reduce-scatter.3.cloned.1.call-start = ((), (), s32[]{:S(2)}) async-start(), calls=%async_computation.4 | async-start | bytes 2621440 | tf_op jit(solution)/shard_map/reduce_scatter | solution.py:83
  6.5 11.4 %copy-start.6 = (bf16[512,2048]{1,0:T(8,128)(2,1)S(1)}, bf16[512,2048]{1,0:T(8,128)(2,1)}, u32[]{:S(2)}) copy-start(bf16[512,2048]{1,0:T(8,128)(2,1)} %param.16) | copy-start | bytes 6291460
  7.4 10.5 %collective-permute-start = (bf16[2,512]{1,0:T(2,128)(2,1)S(1)}, bf16[2,512]{1,0:T(2,128)(2,1)S(1)}, u32[]{:S(2)}, u32[]{:S(2)}) collective-permute-start(bf16[2,512]{1,0:T(2,128)(2,1)S(1)} %slice.28), channel_id=1, source_target_pairs={{0,4},{4,8},{8,12},{12,16},{16,20},{20,24},{24,28},{1,5},{5,9},{9,... | collective-permute-start | bytes 6152 | tf_op jit(solution)/shard_map/ppermute | solution.py:10
  13.1 4.8 %collective-permute-start.1 = (bf16[2,512]{1,0:T(2,128)(2,1)S(1)}, bf16[2,512]{1,0:T(2,128)(2,1)S(1)}, u32[]{:S(2)}, u32[]{:S(2)}) collective-permute-start(bf16[2,512]{1,0:T(2,128)(2,1)S(1)} %slice.29), channel_id=1, source_target_pairs={{0,4},{4,8},{8,12},{12,16},{16,20},{20,24},{24,28},{1,5},{5,9},{9,... | collective-permute-start | bytes 6152 | tf_op jit(solution)/shard_map/ppermute | solution.py:10
  21.8 33.2 %copy-start.1 = (bf16[128,2048]{1,0:T(8,128)(2,1)S(1)}, bf16[128,2048]{1,0:T(8,128)(2,1)}, u32[]{:S(2)}) copy-start(bf16[128,2048]{1,0:T(8,128)(2,1)} %param.17) | copy-start | bytes 1572868
  21.8 34.5 %copy-start.3 = (f32[2048]{0:T(1024)S(1)}, f32[2048]{0:T(1024)}, u32[]{:S(2)}) copy-start(f32[2048]{0:T(1024)} %param.18) | copy-start | bytes 24580
  21.8 149.4 %all-gather.2.cloned.1.call-start = ((), (), s32[]{:S(2)}) async-start(), calls=%async_computation.5 | async-start | bytes 10485760 | tf_op jit(solution)/shard_map/all_gather | solution.py:95
  114.7 147.8 %reduce-scatter.5.cloned.1.call-start = ((), (), s32[]{:S(2)}) async-start(), calls=%async_computation.6 | async-start | bytes 10485760 | tf_op jit(solution)/shard_map/reduce_scatter | solution.py:104
  171.2 7.7 %copy-start.5 = (bf16[4,8,64,2048]{3,2,1,0:T(8,128)(2,1)S(1)}, bf16[4,8,64,2048]{3,2,1,0:T(8,128)(2,1)}, u32[]{:S(2)}) copy-start(bf16[4,8,64,2048]{3,2,1,0:T(8,128)(2,1)} %all-gather.2.cloned.1.call-done) | copy-start | bytes 25165828
  171.2 7.7 %copy-start.7 = (bf16[1,2048,512]{2,1,0:T(8,128)(2,1)S(1)}, bf16[1,2048,512]{2,1,0:T(8,128)(2,1)}, u32[]{:S(2)}) copy-start(bf16[1,2048,512]{2,1,0:T(8,128)(2,1)} %param.22) | copy-start | bytes 6291460
  262.5 53.7 %all-to-all-start.1 = ((bf16[8,64,2048]{2,1,0:T(8,128)(2,1)}), bf16[8,64,2048]{2,1,0:T(8,128)(2,1)}, u32[]{:S(2)}, u32[]{:S(2)}) async-start(bf16[8,64,2048]{2,1,0:T(8,128)(2,1)} %bitcast.41), calls=%async_computation.3 | async-start | bytes 4194304 | tf_op jit(solution)/shard_map/all_to_all | solution.py:112
  324.8 4.9 %copy-start.2 = (bf16[128,2048]{1,0:T(8,128)(2,1)S(1)}, bf16[128,2048]{1,0:T(8,128)(2,1)}, u32[]{:S(2)}) copy-start(bf16[128,2048]{1,0:T(8,128)(2,1)} %reduce-scatter.3.cloned.1.call-done) | copy-start | bytes 1572868
Sparse Core Ops, SparseCore 0:
  22.0 32.9 reduce-scatter.2
  114.8 56.3 all-gather.1
  191.0 71.3 reduce-scatter.4
where the time goes:
time: 338 us; the launch traced here: 337 us
  waiting for transfers between devices  204 us (60%)
  blocking collectives  53.7 us (16%)
  matrix products  23.5 us (7%)
  local copies, waits for them, and re-layouts  17.5 us (5%)
  starting transfers between devices  14 us (4%)
  between operations  13.4 us (4%)
  other arithmetic  10.6 us (3%)
    reduce_scatter x1, waiting for transfers between devices, body(): lax.psum_scatter(rounded(jnp.dot(hidden, down_weight, preferred_element_t...  71.5 us
    all_gather x1, waiting for transfers between devices, body(): received = lax.all_gather(own_arrived, 'tp', axis=0, tiled=True)  56.4 us
    all_to_all x1, blocking collectives, body(): lax.all_to_all(outgoing, 'sp', split_axis=1, concat_axis=1, tiled=True)  53.7 us
    all_to_all x1, waiting for transfers between devices, body(): lax.all_to_all(expert_rows.reshape(groups, capacity, model_width), 'sp',...  47.2 us
    reduce_scatter x1, waiting for transfers between devices, body(): lax.psum_scatter(rounded(jnp.dot(row_block, proj_weight, preferred_elemen...  29.2 us
    ppermute x2, starting transfers between devices, passed_along(): return lax.ppermute(shard, axis, pairs)  8.43 us
    dot_general x1, matrix products, body(): jnp.dot(row_block, gate_weight, preferred_element_type=jnp.float32)  7.67 us
    dot_general x1, matrix products, body(): jnp.dot(hidden, down_weight, preferred_element_type=jnp.float32)  6.79 us
  transfers between devices with their start and end apart: 6, of which 4 were waited for; matrix products, arithmetic and copies ran while one was open for 2% of the time, Pallas kernels for 0%

commit v1 on v0

--- a/solution.py
+++ b/solution.py
@@ -1,6 +1,10 @@
+import functools
+
 import jax
 import jax.numpy as jnp
 from jax import lax
+from jax.experimental import pallas as pl
+from jax.experimental.pallas import tpu as pltpu
 from jax.sharding import PartitionSpec as P
 
 
@@ -29,21 +33,225 @@
     return (hidden_rows * inverse * norm_gain).astype(jnp.bfloat16)
 
 
-def dispatch_rows(normed, route_ids, block_rows, expert_count, capacity):
-    row_count = route_ids.shape[0]
-    top_count = route_ids.shape[1]
-    block_count = row_count // block_rows
-    slots = slot_numbers(route_ids, block_rows, expert_count)
-    row_ids = jnp.arange(row_count, dtype=jnp.int32)
-    flat_index = ((row_ids // block_rows)[:, None] * expert_count + route_ids) * capacity + slots
-    slot_token = (
-        jnp.full((block_count * expert_count * capacity,), row_count, jnp.int32)
-        .at[flat_index.reshape(-1)]
-        .set(jnp.repeat(row_ids, top_count))
-    )
-    padded_rows = jnp.concatenate([normed, jnp.zeros((1, normed.shape[1]), jnp.bfloat16)], axis=0)
-    outgoing = padded_rows[slot_token].reshape(block_count, expert_count, capacity, normed.shape[1])
-    return (outgoing, slots)
+def dispatch_rows(normed, flat_pick, slot_count):
+    slot_ids = jnp.arange(slot_count, dtype=jnp.int32)
+    chosen = jnp.any(flat_pick[None, :, :] == slot_ids[:, None, None], axis=2)
+    return jnp.dot(
+        chosen.astype(jnp.bfloat16), normed, preferred_element_type=jnp.float32
+    ).astype(jnp.bfloat16)
+
+
+MESH = pl.DeviceIdType.MESH
+
+
+def expert_kernel(
+    n, tp, out_ref, gate_hbm, up_hbm, down_hbm, ret_ref,
+    recv, part, mrecv, psum, xrecv, fin, gate_w, up_w, down_w, hid, local_sem, send, got,
+):
+    s = lax.axis_index("sp")
+    t = lax.axis_index("tp")
+    mate = t + 1 - 2 * (t % 2)
+    across = (t + 2) % tp
+    mate_across = (mate + 2) % tp
+    cap, width = out_ref.shape[1], out_ref.shape[2]
+    units = gate_w.shape[1]
+    rows = tp * cap
+
+    weight_copies = [
+        pltpu.make_async_copy(src, dst, local_sem.at[i])
+        for i, (src, dst) in enumerate(
+            [(gate_hbm, gate_w), (up_hbm, up_w), (down_hbm, down_w)]
+        )
+    ]
+    for copy in weight_copies:
+        copy.start()
+
+    barrier = pltpu.get_barrier_semaphore()
+
+    @pl.loop(1, n)
+    def _(k):
+        pl.semaphore_signal(barrier, inc=1, device_id=((s + k) % n, t), device_id_type=MESH)
+
+    for peer in (mate, across):
+        pl.semaphore_signal(barrier, inc=1, device_id=(s, peer), device_id_type=MESH)
+    pl.semaphore_wait(barrier, n + 1)
+
+    def remote(src, dst, lane, k, device):
+        return pltpu.make_async_remote_copy(
+            src_ref=src,
+            dst_ref=dst,
+            send_sem=send.at[lane, k],
+            recv_sem=got.at[lane, k],
+            device_id=device,
+            device_id_type=MESH,
+        )
+
+    def outward(k):
+        to = (s + k) % n
+        return remote(out_ref.at[to], recv.at[k, t], 0, k, (to, t))
+
+    def over(k, block):
+        return remote(recv.at[k, block], recv.at[k, block], 1, k, (s, across))
+
+    def pair_own(k, block):
+        return remote(recv.at[k, block], recv.at[k, block], 2, k, (s, mate))
+
+    def pair_far(k, block):
+        return remote(recv.at[k, block], recv.at[k, block], 3, k, (s, mate))
+
+    def part_near(k):
+        return remote(part.at[k, mate], mrecv.at[k, 0], 4, k, (s, mate))
+
+    def part_far(k):
+        return remote(part.at[k, mate_across], mrecv.at[k, 1], 5, k, (s, mate))
+
+    def sum_over(k):
+        return remote(psum.at[k], xrecv.at[k], 6, k, (s, across))
+
+    def homeward(k):
+        return remote(fin.at[k], ret_ref.at[s], 7, k, ((s + n - k) % n, t))
+
+    own = pltpu.make_async_copy(out_ref.at[s], recv.at[0, t], local_sem.at[3])
+    own.start()
+
+    @pl.loop(1, n)
+    def _(k):
+        outward(k).start()
+
+    own.wait()
+
+    def ffn(k):
+        def load():
+            block = recv[k]
+            if cap % 16:
+                return block.astype(jnp.float32).reshape(rows, width).astype(jnp.bfloat16)
+            return block.reshape(rows, width)
+
+        cols = min(256, units)
+
+        @pl.loop(0, units // cols)
+        def _(c):
+            at = pl.ds(pl.multiple_of(c * cols, cols), cols)
+            x = load()
+            gate = jnp.dot(x, gate_w[:, at], preferred_element_type=jnp.float32)
+            up = jnp.dot(x, up_w[:, at], preferred_element_type=jnp.float32)
+            hid[:, at] = (gate / (1.0 + jnp.exp(-gate)) * up).astype(jnp.bfloat16)
+
+        wide = min(512, width)
+
+        @pl.loop(0, width // wide)
+        def _(c):
+            at = pl.ds(pl.multiple_of(c * wide, wide), wide)
+            y = jnp.dot(hid[...], down_w[:, at], preferred_element_type=jnp.float32)
+            part[k, :, :, at] = y.reshape(tp, cap, wide).astype(jnp.bfloat16)
+
+    def wide_sum(*blocks):
+        total = blocks[0].astype(jnp.float32)
+        for block in blocks[1:]:
+            total = total + block.astype(jnp.float32)
+        return total
+
+    @pl.loop(0, n + 4)
+    def _(i):
+        @pl.when(i < n)
+        def _():
+            @pl.when(i > 0)
+            def _():
+                outward(i).wait_recv()
+
+            over(i, t).start()
+            pair_own(i, t).start()
+
+        @pl.when((i >= 1) & (i < n + 1))
+        def _():
+            k = i - 1
+            over(k, across).wait_recv()
+            pair_far(k, across).start()
+
+        @pl.when(i == 2)
+        def _():
+            for copy in weight_copies:
+                copy.wait()
+
+        @pl.when((i >= 2) & (i < n + 2))
+        def _():
+            k = i - 2
+            pair_own(k, mate).wait_recv()
+            pair_far(k, mate_across).wait_recv()
+            ffn(k)
+            part_far(k).start()
+            part_near(k).start()
+
+        @pl.when((i >= 3) & (i < n + 3))
+        def _():
+            k = i - 3
+            part_far(k).wait_recv()
+            psum[k] = wide_sum(part[k, across], mrecv[k, 1]).astype(jnp.bfloat16)
+            sum_over(k).start()
+
+        @pl.when(i >= 4)
+        def _():
+            k = i - 4
+            part_near(k).wait_recv()
+            sum_over(k).wait_recv()
+            total = wide_sum(part[k, t], mrecv[k, 0], xrecv[k]).astype(jnp.bfloat16)
+
+            @pl.when(k == 0)
+            def _():
+                ret_ref[s] = total
+
+            @pl.when(k > 0)
+            def _():
+                fin[k] = total
+                homeward(k).start()
+
+    @pl.loop(0, n)
+    def _(k):
+        over(k, t).wait_send()
+        pair_own(k, t).wait_send()
+        pair_far(k, across).wait_send()
+        part_near(k).wait_send()
+        part_far(k).wait_send()
+        sum_over(k).wait_send()
+
+        @pl.when(k > 0)
+        def _():
+            outward(k).wait_send()
+            homeward(k).wait_send()
+            homeward(k).wait_recv()
+
+
+def run_experts(outgoing, gate_weight, up_weight, down_weight):
+    n, cap, width = outgoing.shape
+    tp = lax.axis_size("tp")
+    units = gate_weight.shape[1]
+    vmem = pl.BlockSpec(memory_space=pltpu.VMEM)
+    hbm = pl.BlockSpec(memory_space=pl.ANY)
+    bf16 = jnp.bfloat16
+    return pl.pallas_call(
+        functools.partial(expert_kernel, n, tp),
+        out_shape=jax.ShapeDtypeStruct((n, cap, width), bf16),
+        in_specs=[vmem, hbm, hbm, hbm],
+        out_specs=vmem,
+        scratch_shapes=[
+            pltpu.VMEM((n, tp, cap, width), bf16),
+            pltpu.VMEM((n, tp, cap, width), bf16),
+            pltpu.VMEM((n, 2, cap, width), bf16),
+            pltpu.VMEM((n, cap, width), bf16),
+            pltpu.VMEM((n, cap, width), bf16),
+            pltpu.VMEM((n, cap, width), bf16),
+            pltpu.VMEM(gate_weight.shape, bf16),
+            pltpu.VMEM(up_weight.shape, bf16),
+            pltpu.VMEM(down_weight.shape, bf16),
+            pltpu.VMEM((tp * cap, units), bf16),
+            pltpu.SemaphoreType.DMA((4,)),
+            pltpu.SemaphoreType.DMA((8, n)),
+            pltpu.SemaphoreType.DMA((8, n)),
+        ],
+        compiler_params=pltpu.CompilerParams(
+            collective_id=1, has_side_effects=True, vmem_limit_bytes=60 * 1024 * 1024
+        ),
+    )(outgoing, gate_weight, up_weight, down_weight)
 
 
 def body(
@@ -90,36 +298,24 @@
     ).astype(jnp.float32)
     my_rows = residual.astype(jnp.float32) + summed
     normed = normalize(my_rows, norm_gain)
-    outgoing, own_slots = dispatch_rows(normed, own_routes, quarter, groups, capacity)
-    own_arrived = lax.all_to_all(outgoing, "sp", split_axis=1, concat_axis=1, tiled=True)
-    received = lax.all_gather(own_arrived, "tp", axis=0, tiled=True)
-    flat_rows = received.reshape(tp_count * groups * capacity, model_width)
-    gate_weight = expert_gate[0]
-    up_weight = expert_up[0]
-    down_weight = expert_down[0]
-    row_block = flat_rows
-    gate_pre = jnp.dot(row_block, gate_weight, preferred_element_type=jnp.float32)
-    up_pre = jnp.dot(row_block, up_weight, preferred_element_type=jnp.float32)
-    hidden = (jax.nn.silu(gate_pre) * up_pre).astype(jnp.bfloat16)
-    expert_rows = lax.psum_scatter(
-        rounded(jnp.dot(hidden, down_weight, preferred_element_type=jnp.float32)).astype(
-            jnp.bfloat16
-        ),
-        "tp",
-        scatter_dimension=0,
-        tiled=True,
-    )
-    returned = lax.all_to_all(
-        expert_rows.reshape(groups, capacity, model_width),
-        "sp",
-        split_axis=0,
-        concat_axis=0,
-        tiled=True,
-    )
+    own_slots = slot_numbers(own_routes, quarter, groups)
     flat_pick = own_routes * capacity + own_slots
-    picked = returned.reshape(groups * capacity, model_width)[flat_pick]
-    weighted = jnp.sum(own_weights[:, :, None] * picked.astype(jnp.float32), axis=1)
-    return (my_rows + weighted).astype(jnp.bfloat16)
+    slot_count = groups * capacity
+    outgoing = dispatch_rows(normed, flat_pick, slot_count)
+    returned = run_experts(
+        outgoing.reshape(groups, capacity, model_width),
+        expert_gate[0],
+        expert_up[0],
+        expert_down[0],
+    ).reshape(slot_count, model_width)
+    total = my_rows
+    for k in range(top_count):
+        pick = flat_pick[:, k, None] == jnp.arange(slot_count, dtype=jnp.int32)
+        picked = jnp.dot(
+            pick.astype(jnp.bfloat16), returned, preferred_element_type=jnp.float32
+        )
+        total = total + own_weights[:, k, None] * picked
+    return total.astype(jnp.bfloat16)
 
 
 def solution(mesh):

time: 338 us -> 204 us (0.60)
  waiting for transfers between devices: 204 us -> 30 us
  Pallas kernels: 0 us -> 135 us
  blocking collectives: 53.7 us -> 0 us
  matrix products: 23.5 us -> 9.48 us
  local copies, waits for them, and re-layouts: 17.5 us -> 3.89 us
  other arithmetic: 10.6 us -> 3.45 us
  starting transfers between devices: 14 us -> 8.31 us
    pallas_call x0 -> x1, Pallas kernels: none -> 135 us  [run_experts(): pl.pallas_call(functools.partial(expert_kernel, n, tp), out_shape=jax.Sha...]
    reduce_scatter x1 -> x0, waiting for transfers between devices: 71.5 us -> none  [body(): lax.psum_scatter(rounded(jnp.dot(hidden, down_weight, preferred_element_t...]
    all_gather x1 -> x0, waiting for transfers between devices: 56.4 us -> none  [body(): received = lax.all_gather(own_arrived, 'tp', axis=0, tiled=True)]
    all_to_all x1 -> x0, blocking collectives: 53.7 us -> none  [body(): lax.all_to_all(outgoing, 'sp', split_axis=1, concat_axis=1, tiled=True)]
    all_to_all x1 -> x0, waiting for transfers between devices: 47.2 us -> none  [body(): lax.all_to_all(expert_rows.reshape(groups, capacity, model_width), 'sp',...]
    dot_general x3, matrix products: 19.6 us -> 6.7 us  [the longest x2 3.58 us: body(): jnp.dot(pick.astype(jnp.bfloat16), returned, preferred_element_type=jnp.f...]
    gather x2 -> x0, local copies, waits for them, and re-layouts: 8.55 us -> none  [the longest x1 5.21 us: body(): picked = returned.reshape(groups * capacity, model_width)[flat_pick]]
    all_to_all x1 -> x0, starting transfers between devices: 5.52 us -> none  [body(): lax.all_to_all(expert_rows.reshape(groups, capacity, model_width), 'sp',...]
  transfers between devices with their start and end apart: 6 -> 3, of which waited for: 4 -> 1; matrix products, arithmetic and copies ran while one was open for 2% -> 3% of each run, Pallas kernels for 0% -> 0%
where the time goes in v1:
time: 204 us
  Pallas kernels  135 us (66%)
  waiting for transfers between devices  30 us (15%)
  between operations  13.6 us (7%)
  matrix products  9.48 us (5%)
  starting transfers between devices  8.31 us (4%)
  local copies, waits for them, and re-layouts  3.89 us (2%)
  other arithmetic  3.45 us (2%)
    pallas_call x1, Pallas kernels, run_experts(): pl.pallas_call(functools.partial(expert_kernel, n, tp), out_shape=jax.Sha...  135 us
    reduce_scatter x1, waiting for transfers between devices, body(): lax.psum_scatter(rounded(jnp.dot(row_block, proj_weight, preferred_elemen...  30 us
    ppermute x2, starting transfers between devices, passed_along(): return lax.ppermute(shard, axis, pairs)  8.3 us
  transfers between devices with their start and end apart: 3, of which 1 were waited for; matrix products, arithmetic and copies ran while one was open for 3% of the time, Pallas kernels for 0%

profile of v1, /device:TPU:0, one launch (start us, length us, event | category | flops | bytes accessed | tf_op | source)
XLA Modules:
  0.0 203.5 jit_solution(7453195664342104744)
XLA Ops:
  6.5 0.0 copy-start
  6.5 0.0 reduce-scatter.2.cloned.1.call-start
  6.5 0.9 slice.41
  7.4 4.9 %collective-permute-start.1 = (bf16[2,512]{1,0:T(2,128)(2,1)S(1)}, bf16[2,512]{1,0:T(2,128)(2,1)S(1)}, u32[]{:S(2)}, u32[]{:S(2)}) collective-permute-start(bf16[2,512]{1,0:T(2,128)(2,1)S(1)} %slice.41), channel_id=1, source_target_pairs={{0,4},{4,8},{8,12},{12,16},{16,20},{20,24},{24,28},{1,5},{5,9},{9,... | collective-permute-start | bytes 6152 | tf_op jit(solution)/shard_map/ppermute | solution.py:14
  12.3 0.7 slice.40
  13.0 3.4 %collective-permute-start = (bf16[2,512]{1,0:T(2,128)(2,1)S(1)}, bf16[2,512]{1,0:T(2,128)(2,1)S(1)}, u32[]{:S(2)}, u32[]{:S(2)}) collective-permute-start(bf16[2,512]{1,0:T(2,128)(2,1)S(1)} %slice.40), channel_id=1, source_target_pairs={{0,4},{4,8},{8,12},{12,16},{16,20},{20,24},{24,28},{1,5},{5,9},{9,... | collective-permute-start | bytes 6152 | tf_op jit(solution)/shard_map/ppermute | solution.py:14
  16.4 1.3 convert_multiply_fusion
  17.8 0.0 copy-done.5
  17.8 0.0 collective-permute-done.1
  17.8 0.0 collective-permute-done
  17.8 0.0 copy-done
  17.9 0.0 copy-done.6
  17.9 2.8 %convolution_convert_fusion.1 = bf16[512,2048]{1,0:T(8,128)(2,1)} fusion(bf16[512,2048]{1,0:T(8,128)(2,1)S(1)} %copy-done, f32[2,512]{1,0:T(2,128)S(1)} %convert_multiply_fusion.1, f32[512,512]{1,0:T(8,128)S(1)} %convert_multiply_fusion, bf16[512,512]{1,0:T(8,128)(2,1)S(1)} %copy-done.6, f32[512]{0:T(512)S(1)} %bitcast.39, f32[512]{0:T(512)S(1)} %bitcast.40, ...), kind=kOutput, calls=%fused_computation.1 | convolution fusion | flops 1077411840 | bytes 5777408 | tf_op jit(solution)/shard_map/dot_general | solution.py:292
  20.6 0.0 reduce-scatter.2.cloned.1.call-update
  20.7 0.7 constant_dynamic-slice_fusion
  21.4 0.1 copy.18
  21.5 0.1 eq.70
  21.7 0.6 reduce-window.6
  22.3 0.2 slice_reduce_fusion.2
  22.5 0.1 fusion.20
  22.6 0.1 reshape.140
  22.8 0.1 copy.17
  22.8 0.7 constant_dynamic-slice_fusion.1
  23.5 0.2 slice_reduce_fusion
  23.7 0.1 fusion.16
  23.8 30.0 %reduce-scatter.2.cloned.1.call-done = bf16[128,2048]{1,0:T(8,128)(2,1)} async-done(((bf16[512,2048]{1,0:T(8,128)(2,1)}), bf16[128,2048]{1,0:T(8,128)(2,1)}) %reduce-scatter.2.cloned.1.call-update) | async-done | bytes 524304 | tf_op jit(solution)/shard_map/reduce_scatter | solution.py:291
  53.8 1.3 multiply_reduce_fusion
  55.1 3.1 %convolution_convert_fusion = bf16[512,2048]{1,0:T(8,128)(2,1)} fusion(pred[512,128]{1,0:T(8,128)(4,1)S(1)} %fusion.16, bf16[128,2048]{1,0:T(8,128)(2,1)} %reduce-scatter.2.cloned.1.call-done, bf16[128,2048]{1,0:T(8,128)(2,1)S(1)} %copy-done.2, f32[2048]{0:T(1024)S(1)} %copy-done.4, f32[128]{0:T(128)S(1)} %add_rsqrt_fusion), kind=kOutput, calls=%fused_computation | convolution fusion | flops 271056896 | bytes 3219968 | tf_op jit(solution)/shard_map/dot_general | solution.py:39
  58.2 134.8 %shard_map.118 = bf16[8,64,2048]{2,1,0:T(8,128)(2,1)} custom-call(bf16[8,64,2048]{2,1,0:T(8,128)(2,1)} %bitcast.33, bf16[2048,512]{1,0:T(8,128)(2,1)} %bitcast.34, bf16[2048,512]{1,0:T(8,128)(2,1)} %bitcast.35, bf16[512,2048]{1,0:T(8,128)(2,1)} %bitcast.36), custom_call_target="tpu_custom_call" | custom-call | tf_op jit(solution)/shard_map/pallas_call | solution.py:231
  193.1 2.3 %fusion.1 = f32[128,2048]{1,0:T(8,128)S(1)} fusion(bf16[512,2048]{1,0:T(8,128)(2,1)} %bitcast.31, bf16[128,2048]{1,0:T(8,128)(2,1)S(1)} %copy-done.3, bf16[128,2048]{1,0:T(8,128)(2,1)S(1)} %copy-done.2, f32[128]{0:T(128)S(1)} %get-tuple-element.11, s32[128]{0:T(128)S(1)} %get-tuple-element.6), kind=kOutput, calls=%fused_computation.5 | convolution fusion | flops 269811712 | bytes 4195328 | tf_op jit(solution)/shard_map/dot_general | solution.py:314
  195.4 0.0 copy-done.1
  195.4 1.3 fusion.2
  (17 shorter events, 0.1 us)
Async XLA Ops:
  6.5 11.3 %copy-start = (bf16[512,2048]{1,0:T(8,128)(2,1)S(1)}, bf16[512,2048]{1,0:T(8,128)(2,1)}, u32[]{:S(2)}) copy-start(bf16[512,2048]{1,0:T(8,128)(2,1)} %param.16) | copy-start | bytes 6291460
  6.5 11.2 %copy-start.5 = (f32[3,512]{1,0:T(4,128)S(1)}, f32[3,512]{1,0:T(4,128)}, u32[]{:S(2)}) copy-start(f32[3,512]{1,0:T(4,128)} %param.15) | copy-start | bytes 18436
  6.5 11.3 %copy-start.6 = (bf16[512,512]{1,0:T(8,128)(2,1)S(1)}, bf16[512,512]{1,0:T(8,128)(2,1)}, u32[]{:S(2)}) copy-start(bf16[512,512]{1,0:T(8,128)(2,1)} %param.14) | copy-start | bytes 1572868
  6.5 47.3 %reduce-scatter.2.cloned.1.call-start = ((), (), s32[]{:S(2)}) async-start(), calls=%async_computation.1 | async-start | bytes 2621440 | tf_op jit(solution)/shard_map/reduce_scatter | solution.py:291
  7.4 10.4 %collective-permute-start.1 = (bf16[2,512]{1,0:T(2,128)(2,1)S(1)}, bf16[2,512]{1,0:T(2,128)(2,1)S(1)}, u32[]{:S(2)}, u32[]{:S(2)}) collective-permute-start(bf16[2,512]{1,0:T(2,128)(2,1)S(1)} %slice.41), channel_id=1, source_target_pairs={{0,4},{4,8},{8,12},{12,16},{16,20},{20,24},{24,28},{1,5},{5,9},{9,... | collective-permute-start | bytes 6152 | tf_op jit(solution)/shard_map/ppermute | solution.py:14
  13.0 4.8 %collective-permute-start = (bf16[2,512]{1,0:T(2,128)(2,1)S(1)}, bf16[2,512]{1,0:T(2,128)(2,1)S(1)}, u32[]{:S(2)}, u32[]{:S(2)}) collective-permute-start(bf16[2,512]{1,0:T(2,128)(2,1)S(1)} %slice.40), channel_id=1, source_target_pairs={{0,4},{4,8},{8,12},{12,16},{16,20},{20,24},{24,28},{1,5},{5,9},{9,... | collective-permute-start | bytes 6152 | tf_op jit(solution)/shard_map/ppermute | solution.py:14
  20.6 33.2 %copy-start.2 = (bf16[128,2048]{1,0:T(8,128)(2,1)S(1)}, bf16[128,2048]{1,0:T(8,128)(2,1)}, u32[]{:S(2)}) copy-start(bf16[128,2048]{1,0:T(8,128)(2,1)} %param.17) | copy-start | bytes 1572868
  20.6 34.5 %copy-start.4 = (f32[2048]{0:T(1024)S(1)}, f32[2048]{0:T(1024)}, u32[]{:S(2)}) copy-start(f32[2048]{0:T(1024)} %param.18) | copy-start | bytes 24580
  58.2 134.8 %copy-start.3 = (bf16[128,2048]{1,0:T(8,128)(2,1)S(1)}, bf16[128,2048]{1,0:T(8,128)(2,1)}, u32[]{:S(2)}) copy-start(bf16[128,2048]{1,0:T(8,128)(2,1)} %reduce-scatter.2.cloned.1.call-done) | copy-start | bytes 1572868
  193.1 2.3 %copy-start.1 = (bf16[8,64,2048]{2,1,0:T(8,128)(2,1)S(1)}, bf16[8,64,2048]{2,1,0:T(8,128)(2,1)}, u32[]{:S(2)}) copy-start(bf16[8,64,2048]{2,1,0:T(8,128)(2,1)} %shard_map.118) | copy-start | bytes 6291460
Sparse Core Ops, SparseCore 0:
  20.8 32.9 reduce-scatter.1

commit v2 on v1

--- a/solution.py
+++ b/solution.py
@@ -6,16 +6,6 @@
 from jax.experimental import pallas as pl
 from jax.experimental.pallas import tpu as pltpu
 from jax.sharding import PartitionSpec as P
-
-
-def passed_along(shard, axis, by):
-    size = lax.axis_size(axis)
-    pairs = [(i, i + by) for i in range(size) if 0 <= i + by < size]
-    return lax.ppermute(shard, axis, pairs)
-
-
-def rounded(values):
-    return lax.optimization_barrier(values.astype(jnp.bfloat16)).astype(jnp.float32)
 
 
 def slot_numbers(route_ids, block_rows, expert_count):
@@ -28,11 +18,6 @@
     return jnp.sum(before * one_hot, axis=2).reshape(route_ids.shape)
 
 
-def normalize(hidden_rows, norm_gain):
-    inverse = lax.rsqrt(jnp.mean(hidden_rows * hidden_rows, axis=-1, keepdims=True) + 1e-05)
-    return (hidden_rows * inverse * norm_gain).astype(jnp.bfloat16)
-
-
 def dispatch_rows(normed, flat_pick, slot_count):
     slot_ids = jnp.arange(slot_count, dtype=jnp.int32)
     chosen = jnp.any(flat_pick[None, :, :] == slot_ids[:, None, None], axis=2)
@@ -42,6 +27,138 @@
 
 
 MESH = pl.DeviceIdType.MESH
+
+
+def mixer_kernel(
+    n, tp, halo, pieces, gate_ref, value_ref, out_gate_ref, taps_ref, proj_ref, res_ref, gain_ref,
+    rows_ref, normed_ref, edge, product, mixed, part, mrecv, psum, xrecv, send, got,
+):
+    s = lax.axis_index("sp")
+    t = lax.axis_index("tp")
+    mate = t + 1 - 2 * (t % 2)
+    across = (t + 2) % tp
+    mate_across = (mate + 2) % tp
+    tokens = gate_ref.shape[0]
+    quarter, width = res_ref.shape
+    piece = quarter // pieces
+    after, before = (s + 1) % n, (s + n - 1) % n
+
+    barrier = pltpu.get_barrier_semaphore()
+    for peer in ((s, mate), (s, across), (after, t), (before, t)):
+        pl.semaphore_signal(barrier, inc=1, device_id=peer, device_id_type=MESH)
+
+    def remote(src, dst, lane, device):
+        return pltpu.make_async_remote_copy(
+            src_ref=src,
+            dst_ref=dst,
+            send_sem=send.at[lane],
+            recv_sem=got.at[lane],
+            device_id=device,
+            device_id_type=MESH,
+        )
+
+    tail = pl.ds(tokens - halo, halo)
+    edges = [
+        remote(ref.at[tail], edge.at[i], i, (after, t))
+        for i, ref in enumerate((gate_ref, value_ref))
+    ]
+    pl.semaphore_wait(barrier, 4)
+    for copy in edges:
+        copy.start()
+
+    body_rows = pl.ds(halo, tokens)
+    product[body_rows] = gate_ref[...].astype(jnp.float32) * value_ref[...].astype(jnp.float32)
+    for copy in edges:
+        copy.wait_recv()
+    prior = edge[0].astype(jnp.float32) * edge[1].astype(jnp.float32)
+    product[pl.ds(0, halo)] = jnp.where(s == 0, 0.0, prior)
+    conv_sum = (
+        taps_ref[0:1] * product[pl.ds(halo - 2, tokens)]
+        + taps_ref[1:2] * product[pl.ds(halo - 1, tokens)]
+        + taps_ref[2:3] * product[body_rows]
+    )
+    mixed[...] = (out_gate_ref[...].astype(jnp.float32) * conv_sum).astype(jnp.bfloat16)
+
+    def project(block, p):
+        first = pl.multiple_of(block * quarter + p * piece, piece)
+        y = jnp.dot(
+            mixed[pl.ds(first, piece)], proj_ref[...], preferred_element_type=jnp.float32
+        )
+        part[block, p] = y.astype(jnp.bfloat16)
+
+    def lane(kind, p):
+        return 2 + kind * pieces + p
+
+    def to_mate(kind, block, p):
+        return remote(part.at[block, p], mrecv.at[kind, p], lane(kind, p), (s, mate))
+
+    def over(p):
+        return remote(psum.at[p], xrecv.at[p], lane(2, p), (s, across))
+
+    def wide(block):
+        return block.astype(jnp.float32)
+
+    for p in range(pieces):
+        project(mate_across, p)
+        to_mate(0, mate_across, p).start()
+    for p in range(pieces):
+        project(across, p)
+        to_mate(0, mate_across, p).wait_recv()
+        psum[p] = (wide(part[across, p]) + wide(mrecv[0, p])).astype(jnp.bfloat16)
+        over(p).start()
+    for p in range(pieces):
+        project(mate, p)
+        to_mate(1, mate, p).start()
+    for p in range(pieces):
+        project(t, p)
+    for p in range(pieces):
+        to_mate(1, mate, p).wait_recv()
+        over(p).wait_recv()
+        at = pl.ds(p * piece, piece)
+        summed = wide(part[t, p]) + wide(mrecv[1, p]) + wide(xrecv[p])
+        hidden_rows = wide(res_ref[at]) + summed
+        inverse = lax.rsqrt(jnp.mean(hidden_rows * hidden_rows, axis=-1, keepdims=True) + 1e-05)
+        rows_ref[at] = hidden_rows
+        normed_ref[at] = (hidden_rows * inverse * gain_ref[...]).astype(jnp.bfloat16)
+    for copy in edges:
+        copy.wait_send()
+    for p in range(pieces):
+        to_mate(0, mate_across, p).wait_send()
+        to_mate(1, mate, p).wait_send()
+        over(p).wait_send()
+
+
+def run_mixer(gate_in, value_in, gate_out, conv_taps, proj_weight, residual, norm_gain):
+    n, tp = lax.axis_size("sp"), lax.axis_size("tp")
+    tokens, channels = gate_in.shape
+    quarter, width = residual.shape
+    halo, pieces = 16, 4
+    piece = quarter // pieces
+    vmem = pl.BlockSpec(memory_space=pltpu.VMEM)
+    bf16, f32 = jnp.bfloat16, jnp.float32
+    return pl.pallas_call(
+        functools.partial(mixer_kernel, n, tp, halo, pieces),
+        out_shape=(
+            jax.ShapeDtypeStruct((quarter, width), f32),
+            jax.ShapeDtypeStruct((quarter, width), bf16),
+        ),
+        in_specs=[vmem] * 7,
+        out_specs=(vmem, vmem),
+        scratch_shapes=[
+            pltpu.VMEM((2, halo, channels), bf16),
+            pltpu.VMEM((halo + tokens, channels), f32),
+            pltpu.VMEM((tokens, channels), bf16),
+            pltpu.VMEM((tp, pieces, piece, width), bf16),
+            pltpu.VMEM((2, pieces, piece, width), bf16),
+            pltpu.VMEM((pieces, piece, width), bf16),
+            pltpu.VMEM((pieces, piece, width), bf16),
+            pltpu.SemaphoreType.DMA((2 + 3 * pieces,)),
+            pltpu.SemaphoreType.DMA((2 + 3 * pieces,)),
+        ],
+        compiler_params=pltpu.CompilerParams(
+            collective_id=2, has_side_effects=True, vmem_limit_bytes=60 * 1024 * 1024
+        ),
+    )(gate_in, value_in, gate_out, conv_taps, proj_weight, residual, norm_gain.reshape(1, width))
 
 
 def expert_kernel(
@@ -268,7 +385,6 @@
     expert_up,
     expert_down,
 ):
-    tok_dev = gate_in.shape[0]
     model_width = residual.shape[1]
     tp_count = lax.axis_size("tp")
     groups = lax.axis_size("sp")
@@ -277,27 +393,11 @@
     capacity = 2 * quarter * top_count // groups
     tp_index = lax.axis_index("tp")
     first_own = tp_index * quarter
-    prior_gate, prior_value = passed_along(
-        (gate_in[tok_dev - 2 :], value_in[tok_dev - 2 :]), "sp", 1
-    )
-    product = gate_in.astype(jnp.float32) * value_in.astype(jnp.float32)
-    prior_mix = prior_gate.astype(jnp.float32) * prior_value.astype(jnp.float32)
-    padded = jnp.concatenate([prior_mix, product], axis=0)
-    conv_sum = conv_taps[0] * padded[:-2] + conv_taps[1] * padded[1:-1] + conv_taps[2] * padded[2:]
-    mixed_out = (gate_out.astype(jnp.float32) * conv_sum).astype(jnp.bfloat16)
     own_routes = lax.dynamic_slice_in_dim(routes, first_own, quarter, 0)
     own_weights = lax.dynamic_slice_in_dim(route_weight, first_own, quarter, 0)
-    row_block = mixed_out
-    summed = lax.psum_scatter(
-        rounded(jnp.dot(row_block, proj_weight, preferred_element_type=jnp.float32)).astype(
-            jnp.bfloat16
-        ),
-        "tp",
-        scatter_dimension=0,
-        tiled=True,
-    ).astype(jnp.float32)
-    my_rows = residual.astype(jnp.float32) + summed
-    normed = normalize(my_rows, norm_gain)
+    my_rows, normed = run_mixer(
+        gate_in, value_in, gate_out, conv_taps, proj_weight, residual, norm_gain
+    )
     own_slots = slot_numbers(own_routes, quarter, groups)
     flat_pick = own_routes * capacity + own_slots
     slot_count = groups * capacity

time: 204 us -> 172 us (0.84)
  waiting for transfers between devices: 30 us -> 0 us
  Pallas kernels: 135 us -> 162 us
  between operations: 13.6 us -> 0.09 us
  starting transfers between devices: 8.31 us -> 0 us
  matrix products: 9.48 us -> 6.64 us
  other arithmetic: 3.45 us -> 0.79 us
    reduce_scatter x1 -> x0, waiting for transfers between devices: 30 us -> none  [body(): lax.psum_scatter(rounded(jnp.dot(row_block, proj_weight, preferred_elemen...]
    pallas_call x0 -> x1, Pallas kernels: none -> 28.5 us  [run_mixer(): pl.pallas_call(functools.partial(mixer_kernel, n, tp, halo, pieces), out_...]
    ppermute x2 -> x0, starting transfers between devices: 8.3 us -> none  [passed_along(): return lax.ppermute(shard, axis, pairs)]
    dot_general x1 -> x0, matrix products: 2.78 us -> none  [body(): jnp.dot(row_block, proj_weight, preferred_element_type=jnp.float32)]
  transfers between devices with their start and end apart: 3 -> 0, of which waited for: 1 -> 0; matrix products, arithmetic and copies ran while one was open for 3% -> 0% of each run, Pallas kernels for 0% -> 0%
where the time goes in v2:
time: 172 us; the launch traced here: 171 us
  Pallas kernels  162 us (94%)
  matrix products  6.64 us (4%)
  local copies, waits for them, and re-layouts  2.25 us (1%)
    pallas_call x1, Pallas kernels, run_experts(): pl.pallas_call(functools.partial(expert_kernel, n, tp), out_shape=jax.Sha...  133 us
    pallas_call x1, Pallas kernels, run_mixer(): pl.pallas_call(functools.partial(mixer_kernel, n, tp, halo, pieces), out_...  28.5 us
    dot_general x2, matrix products, body(): jnp.dot(pick.astype(jnp.bfloat16), returned, preferred_element_type=jnp.f...  3.55 us

profile of v2, /device:TPU:0, one launch (start us, length us, event | category | flops | bytes accessed | tf_op | source)
XLA Modules:
  0.0 171.3 jit_solution(2408838694789275474)
XLA Ops:
  0.0 0.0 copy-start
  0.0 0.7 copy-done
  0.7 0.7 constant_dynamic-slice_fusion.1
  1.4 0.1 copy.18
  1.5 0.1 eq.70
  1.6 0.6 reduce-window.6
  2.2 0.2 slice_reduce_fusion.2
  2.5 0.1 fusion.7
  2.6 0.1 reshape.135
  2.7 0.1 copy.17
  2.8 0.2 slice_reduce_fusion
  3.0 0.1 fusion.3
  3.1 28.5 %shard_map.118 = (f32[128,2048]{1,0:T(8,128)}, bf16[128,2048]{1,0:T(8,128)(2,1)}) custom-call(bf16[512,512]{1,0:T(8,128)(2,1)} %gate_ref.1, bf16[512,512]{1,0:T(8,128)(2,1)} %value_ref.1, bf16[512,512]{1,0:T(8,128)(2,1)} %out_gate_ref.1, f32[3,512]{1,0:T(4,128)} %taps_ref.1, bf16[512,2048]{1,0:T(8,128)(2,1)} %proj_ref.1, bf16[128,2048]{1,0:T(8,128)(2,1)} %res_ref.1, ...), custom_call_target="tpu_custom_call" | custom-call | tf_op jit(solution)/shard_map/pallas_call | solution.py:139
  31.6 3.1 %convolution_convert_fusion = bf16[512,2048]{1,0:T(8,128)(2,1)} fusion(pred[512,128]{1,0:T(8,128)(4,1)S(1)} %fusion.3, bf16[128,2048]{1,0:T(8,128)(2,1)} %get-tuple-element.8), kind=kOutput, calls=%fused_computation | convolution fusion | flops 269484032 | bytes 2686976 | tf_op jit(solution)/shard_map/dot_general | solution.py:24
  34.7 0.0 copy-start.2
  34.7 133.0 %shard_map.119 = bf16[8,64,2048]{2,1,0:T(8,128)(2,1)} custom-call(bf16[8,64,2048]{2,1,0:T(8,128)(2,1)} %bitcast.31, bf16[2048,512]{1,0:T(8,128)(2,1)} %bitcast.32, bf16[2048,512]{1,0:T(8,128)(2,1)} %bitcast.33, bf16[512,2048]{1,0:T(8,128)(2,1)} %bitcast.34), custom_call_target="tpu_custom_call" | custom-call | tf_op jit(solution)/shard_map/pallas_call | solution.py:348
  167.8 0.0 copy-done.2
  167.8 0.0 copy-start.1
  167.8 2.3 %fusion.1 = f32[128,2048]{1,0:T(8,128)S(1)} fusion(f32[128,2048]{1,0:T(8,128)S(1)} %copy-done.2, bf16[512,2048]{1,0:T(8,128)(2,1)} %bitcast.29, f32[128]{0:T(128)S(1)} %get-tuple-element.12, s32[128]{0:T(128)S(1)} %get-tuple-element.10), kind=kOutput, calls=%fused_computation.4 | convolution fusion | flops 269025280 | bytes 4195328 | tf_op jit(solution)/shard_map/dot_general | solution.py:414
  170.0 0.0 copy-done.1
  170.0 1.3 fusion.2
  (6 shorter events, 0.1 us)
Async XLA Ops:
  0.0 0.7 copy-start
  34.7 133.0 %copy-start.2 = (f32[128,2048]{1,0:T(8,128)S(1)}, f32[128,2048]{1,0:T(8,128)}, u32[]{:S(2)}) copy-start(f32[128,2048]{1,0:T(8,128)} %get-tuple-element.7) | copy-start | bytes 3145732
  167.8 2.3 %copy-start.1 = (bf16[8,64,2048]{2,1,0:T(8,128)(2,1)S(1)}, bf16[8,64,2048]{2,1,0:T(8,128)(2,1)}, u32[]{:S(2)}) copy-start(bf16[8,64,2048]{2,1,0:T(8,128)(2,1)} %shard_map.119) | copy-start | bytes 6291460

commit v3 on v2

--- a/solution.py
+++ b/solution.py
@@ -162,7 +162,7 @@
 
 
 def expert_kernel(
-    n, tp, out_ref, gate_hbm, up_hbm, down_hbm, ret_ref,
+    n, tp, halves, out_ref, gate_hbm, up_hbm, down_hbm, ret_ref,
     recv, part, mrecv, psum, xrecv, fin, gate_w, up_w, down_w, hid, local_sem, send, got,
 ):
     s = lax.axis_index("sp")
@@ -173,6 +173,7 @@
     cap, width = out_ref.shape[1], out_ref.shape[2]
     units = gate_w.shape[1]
     rows = tp * cap
+    steps = n * halves
 
     weight_copies = [
         pltpu.make_async_copy(src, dst, local_sem.at[i])
@@ -204,8 +205,8 @@
         )
 
     def outward(k):
-        to = (s + k) % n
-        return remote(out_ref.at[to], recv.at[k, t], 0, k, (to, t))
+        to = (s + k // halves) % n
+        return remote(out_ref.at[to * halves + k % halves], recv.at[k, t], 0, k, (to, t))
 
     def over(k, block):
         return remote(recv.at[k, block], recv.at[k, block], 1, k, (s, across))
@@ -226,16 +227,22 @@
         return remote(psum.at[k], xrecv.at[k], 6, k, (s, across))
 
     def homeward(k):
-        return remote(fin.at[k], ret_ref.at[s], 7, k, ((s + n - k) % n, t))
-
-    own = pltpu.make_async_copy(out_ref.at[s], recv.at[0, t], local_sem.at[3])
-    own.start()
-
-    @pl.loop(1, n)
+        to = (s + n - k // halves) % n
+        return remote(fin.at[k], ret_ref.at[s * halves + k % halves], 7, k, (to, t))
+
+    own = [
+        pltpu.make_async_copy(out_ref.at[s * halves + h], recv.at[h, t], local_sem.at[3 + h])
+        for h in range(halves)
+    ]
+    for copy in own:
+        copy.start()
+
+    @pl.loop(halves, steps)
     def _(k):
         outward(k).start()
 
-    own.wait()
+    for copy in own:
+        copy.wait()
 
     def ffn(k):
         def load():
@@ -268,29 +275,52 @@
             total = total + block.astype(jnp.float32)
         return total
 
-    @pl.loop(0, n + 4)
+    @pl.loop(0, steps + 4)
     def _(i):
-        @pl.when(i < n)
-        def _():
-            @pl.when(i > 0)
+        @pl.when(i < steps)
+        def _():
+            @pl.when(i >= halves)
             def _():
                 outward(i).wait_recv()
 
             over(i, t).start()
             pair_own(i, t).start()
 
-        @pl.when((i >= 1) & (i < n + 1))
+        @pl.when((i >= 1) & (i < steps + 1))
         def _():
             k = i - 1
             over(k, across).wait_recv()
             pair_far(k, across).start()
 
+        @pl.when((i >= 3) & (i < steps + 3))
+        def _():
+            k = i - 3
+            part_far(k).wait_recv()
+            psum[k] = wide_sum(part[k, across], mrecv[k, 1]).astype(jnp.bfloat16)
+            sum_over(k).start()
+
+        @pl.when(i >= 4)
+        def _():
+            k = i - 4
+            part_near(k).wait_recv()
+            sum_over(k).wait_recv()
+            total = wide_sum(part[k, t], mrecv[k, 0], xrecv[k]).astype(jnp.bfloat16)
+
+            @pl.when(k < halves)
+            def _():
+                ret_ref[s * halves + k] = total
+
+            @pl.when(k >= halves)
+            def _():
+                fin[k] = total
+                homeward(k).start()
+
         @pl.when(i == 2)
         def _():
             for copy in weight_copies:
                 copy.wait()
 
-        @pl.when((i >= 2) & (i < n + 2))
+        @pl.when((i >= 2) & (i < steps + 2))
         def _():
             k = i - 2
             pair_own(k, mate).wait_recv()
@@ -299,30 +329,7 @@
             part_far(k).start()
             part_near(k).start()
 
-        @pl.when((i >= 3) & (i < n + 3))
-        def _():
-            k = i - 3
-            part_far(k).wait_recv()
-            psum[k] = wide_sum(part[k, across], mrecv[k, 1]).astype(jnp.bfloat16)
-            sum_over(k).start()
-
-        @pl.when(i >= 4)
-        def _():
-            k = i - 4
-            part_near(k).wait_recv()
-            sum_over(k).wait_recv()
-            total = wide_sum(part[k, t], mrecv[k, 0], xrecv[k]).astype(jnp.bfloat16)
-
-            @pl.when(k == 0)
-            def _():
-                ret_ref[s] = total
-
-            @pl.when(k > 0)
-            def _():
-                fin[k] = total
-                homeward(k).start()
-
-    @pl.loop(0, n)
+    @pl.loop(0, steps)
     def _(k):
         over(k, t).wait_send()
         pair_own(k, t).wait_send()
@@ -331,7 +338,7 @@
         part_far(k).wait_send()
         sum_over(k).wait_send()
 
-        @pl.when(k > 0)
+        @pl.when(k >= halves)
         def _():
             outward(k).wait_send()
             homeward(k).wait_send()
@@ -342,33 +349,35 @@
     n, cap, width = outgoing.shape
     tp = lax.axis_size("tp")
     units = gate_weight.shape[1]
+    halves = 2 if cap % 32 == 0 else 1
+    steps, cap = n * halves, cap // halves
     vmem = pl.BlockSpec(memory_space=pltpu.VMEM)
     hbm = pl.BlockSpec(memory_space=pl.ANY)
     bf16 = jnp.bfloat16
     return pl.pallas_call(
-        functools.partial(expert_kernel, n, tp),
-        out_shape=jax.ShapeDtypeStruct((n, cap, width), bf16),
+        functools.partial(expert_kernel, n, tp, halves),
+        out_shape=jax.ShapeDtypeStruct((steps, cap, width), bf16),
         in_specs=[vmem, hbm, hbm, hbm],
         out_specs=vmem,
         scratch_shapes=[
-            pltpu.VMEM((n, tp, cap, width), bf16),
-            pltpu.VMEM((n, tp, cap, width), bf16),
-            pltpu.VMEM((n, 2, cap, width), bf16),
-            pltpu.VMEM((n, cap, width), bf16),
-            pltpu.VMEM((n, cap, width), bf16),
-            pltpu.VMEM((n, cap, width), bf16),
+            pltpu.VMEM((steps, tp, cap, width), bf16),
+            pltpu.VMEM((steps, tp, cap, width), bf16),
+            pltpu.VMEM((steps, 2, cap, width), bf16),
+            pltpu.VMEM((steps, cap, width), bf16),
+            pltpu.VMEM((steps, cap, width), bf16),
+            pltpu.VMEM((steps, cap, width), bf16),
             pltpu.VMEM(gate_weight.shape, bf16),
             pltpu.VMEM(up_weight.shape, bf16),
             pltpu.VMEM(down_weight.shape, bf16),
             pltpu.VMEM((tp * cap, units), bf16),
-            pltpu.SemaphoreType.DMA((4,)),
-            pltpu.SemaphoreType.DMA((8, n)),
-            pltpu.SemaphoreType.DMA((8, n)),
+            pltpu.SemaphoreType.DMA((3 + halves,)),
+            pltpu.SemaphoreType.DMA((8, steps)),
+            pltpu.SemaphoreType.DMA((8, steps)),
         ],
         compiler_params=pltpu.CompilerParams(
             collective_id=1, has_side_effects=True, vmem_limit_bytes=60 * 1024 * 1024
         ),
-    )(outgoing, gate_weight, up_weight, down_weight)
+    )(outgoing.reshape(steps, cap, width), gate_weight, up_weight, down_weight)
 
 
 def body(

time: 172 us -> 156 us (0.907)
  Pallas kernels: 162 us -> 146 us
    pallas_call x1, Pallas kernels: 133 us -> 118 us  [run_experts(): pl.pallas_call(functools.partial(expert_kernel, n, tp, halves), out_shape...]
where the time goes in v3:
time: 156 us
  Pallas kernels  146 us (94%)
  matrix products  6.64 us (4%)
  local copies, waits for them, and re-layouts  2.25 us (1%)
    pallas_call x1, Pallas kernels, run_experts(): pl.pallas_call(functools.partial(expert_kernel, n, tp, halves), out_shape...  118 us
    pallas_call x1, Pallas kernels, run_mixer(): pl.pallas_call(functools.partial(mixer_kernel, n, tp, halo, pieces), out_...  28.5 us
    dot_general x2, matrix products, body(): jnp.dot(pick.astype(jnp.bfloat16), returned, preferred_element_type=jnp.f...  3.55 us

profile of v3, /device:TPU:0, one launch (start us, length us, event | category | flops | bytes accessed | tf_op | source)
XLA Modules:
  0.0 156.2 jit_solution(3056335027640439495)
XLA Ops:
  0.0 0.0 copy-start
  0.0 0.7 copy-done
  0.7 0.7 constant_dynamic-slice_fusion.1
  1.4 0.1 copy.18
  1.5 0.1 eq.70
  1.6 0.6 reduce-window.6
  2.2 0.2 slice_reduce_fusion.2
  2.5 0.1 fusion.7
  2.6 0.1 reshape.132
  2.7 0.1 copy.17
  2.8 0.2 slice_reduce_fusion
  3.0 0.1 fusion.3
  3.1 28.5 %shard_map.118 = (f32[128,2048]{1,0:T(8,128)}, bf16[128,2048]{1,0:T(8,128)(2,1)}) custom-call(bf16[512,512]{1,0:T(8,128)(2,1)} %gate_ref.1, bf16[512,512]{1,0:T(8,128)(2,1)} %value_ref.1, bf16[512,512]{1,0:T(8,128)(2,1)} %out_gate_ref.1, f32[3,512]{1,0:T(4,128)} %taps_ref.1, bf16[512,2048]{1,0:T(8,128)(2,1)} %proj_ref.1, bf16[128,2048]{1,0:T(8,128)(2,1)} %res_ref.1, ...), custom_call_target="tpu_custom_call" | custom-call | tf_op jit(solution)/shard_map/pallas_call | solution.py:139
  31.6 3.1 %convolution_convert_fusion = bf16[512,2048]{1,0:T(8,128)(2,1)} fusion(pred[512,128]{1,0:T(8,128)(4,1)S(1)} %fusion.3, bf16[128,2048]{1,0:T(8,128)(2,1)} %get-tuple-element.8), kind=kOutput, calls=%fused_computation | convolution fusion | flops 269484032 | bytes 2686976 | tf_op jit(solution)/shard_map/dot_general | solution.py:24
  34.7 0.0 copy-start.2
  34.7 117.9 %shard_map.119 = bf16[16,32,2048]{2,1,0:T(8,128)(2,1)} custom-call(bf16[16,32,2048]{2,1,0:T(8,128)(2,1)} %bitcast.31, bf16[2048,512]{1,0:T(8,128)(2,1)} %bitcast.32, bf16[2048,512]{1,0:T(8,128)(2,1)} %bitcast.33, bf16[512,2048]{1,0:T(8,128)(2,1)} %bitcast.34), custom_call_target="tpu_custom_call" | custom-call | tf_op jit(solution)/shard_map/pallas_call | solution.py:357
  152.6 0.0 copy-done.2
  152.6 0.0 copy-start.1
  152.6 2.3 %fusion.1 = f32[128,2048]{1,0:T(8,128)S(1)} fusion(f32[128,2048]{1,0:T(8,128)S(1)} %copy-done.2, bf16[512,2048]{1,0:T(8,128)(2,1)} %bitcast.29, f32[128]{0:T(128)S(1)} %get-tuple-element.12, s32[128]{0:T(128)S(1)} %get-tuple-element.10), kind=kOutput, calls=%fused_computation.4 | convolution fusion | flops 269025280 | bytes 4195328 | tf_op jit(solution)/shard_map/dot_general | solution.py:423
  154.9 0.0 copy-done.1
  154.9 1.3 fusion.2
  (6 shorter events, 0.1 us)
Async XLA Ops:
  0.0 0.7 copy-start
  34.7 117.9 %copy-start.2 = (f32[128,2048]{1,0:T(8,128)S(1)}, f32[128,2048]{1,0:T(8,128)}, u32[]{:S(2)}) copy-start(f32[128,2048]{1,0:T(8,128)} %get-tuple-element.7) | copy-start | bytes 3145732
  152.6 2.3 %copy-start.1 = (bf16[16,32,2048]{2,1,0:T(8,128)(2,1)S(1)}, bf16[16,32,2048]{2,1,0:T(8,128)(2,1)}, u32[]{:S(2)}) copy-start(bf16[16,32,2048]{2,1,0:T(8,128)(2,1)} %shard_map.119) | copy-start | bytes 6291460
